TPU v7x, 32 devices: a whole 2x2x4 slice. The times are simulated.
32 devices in a mesh: sp: 8 (over z, y), tp: 4 (over x, core).
Axes of the slice: x: 2, y: 2, z: 4, core: 2. Of those that a mesh axis runs over, the one named last changes fastest.
Arguments:
- inputs: bfloat16 [2, 3072, 4096], P(None, 'sp'), may hold values from -8 to 8
- w_key: bfloat16 [4096, 2048], P(None, 'tp'), may hold values from -0.09375 to 0.09375
- w_value: bfloat16 [4096, 2048], P(None, 'tp'), may hold values from -0.09375 to 0.09375
- w_query: bfloat16 [4096, 2048], P(None, 'tp'), may hold values from -0.09375 to 0.09375
- w_igate: bfloat16 [4096, 16], replicated, may hold values from -1 to 1
- w_fgate: bfloat16 [4096, 16], replicated, may hold values from -0.09375 to 0.09375
- forget_bias: float32 [16], replicated, may hold values from 3 to 12
- new_rows: bfloat16 [2, 4096], P(None, 'tp'), may hold values from -6 to 6
Outputs:
- cache_matrix: bfloat16 [2, 16, 128, 128], P(None, 'tp', 'sp')
- cache_normal: float32 [2, 16, 128], P(None, 'tp', 'sp')
- cache_top: float32 [2, 16], P(None, 'tp')
- read: bfloat16 [2, 16, 128], P(None, 'tp', 'sp')
All inputs are finite; a program needn't handle non-finite values.
Results may differ from a plain program's by a relative error of at most 0.015.
Values may be sent and summed in bfloat16 or wider, within the bound.
A program may use at most 64 MiB of HBM per device.

v0:
```python
import jax
import jax.numpy as jnp
from jax import lax
from jax.sharding import PartitionSpec as P

DH = 128
EPS = 1e-06


def prefix(value, axis, combine, identity):
    devices, here = (lax.axis_size(axis), lax.axis_index(axis))
    everything = lax.all_gather(value, axis)
    start = jnp.broadcast_to(jnp.asarray(identity, value.dtype), value.shape)

    def lap(k, before):
        at = devices - 1 - k
        reached = at > here
        new = combine(before, everything[at])
        return jnp.where(reached, new, before)

    return lax.fori_loop(0, devices, lap, start)


def normalize(row_block):
    scaled = row_block.astype(jnp.float32)
    scaled = scaled * lax.rsqrt(jnp.mean(scaled * scaled, axis=-1, keepdims=True) + EPS)
    return scaled.astype(jnp.bfloat16)


def add_pair(earlier, second):
    return earlier + second


def shards(inputs, w_key, w_value, w_query, w_igate, w_fgate, forget_bias, new_rows):
    head_count = w_key.shape[1] // DH
    seq_count, span, width = inputs.shape
    rows_own = DH // lax.axis_size("sp")
    row_start = lax.axis_index("sp") * rows_own
    head_start = lax.axis_index("tp") * head_count
    gate_in = lax.dynamic_slice_in_dim(w_igate, head_start, head_count, 1)
    gate_forget = lax.dynamic_slice_in_dim(w_fgate, head_start, head_count, 1)
    bias_heads = lax.dynamic_slice_in_dim(forget_bias, head_start, head_count, 0)
    normed = normalize(inputs)
    key_rows = jnp.einsum("spd,dc->spc", normed, w_key, preferred_element_type=jnp.float32).astype(
        jnp.bfloat16
    )
    value_rows = jnp.einsum(
        "spd,dc->spc", normed, w_value, preferred_element_type=jnp.float32
    ).astype(jnp.bfloat16)
    input_pre = jnp.einsum("spd,dh->sph", normed, gate_in, preferred_element_type=jnp.float32)
    log_forget = jax.nn.log_sigmoid(
        jnp.einsum("spd,dh->sph", normed, gate_forget, preferred_element_type=jnp.float32)
        + bias_heads
    )
    running = jnp.cumsum(log_forget, axis=1)
    own_total = running[:, -1, :]
    beyond = prefix(own_total, "sp", add_pair, jnp.zeros_like(own_total))
    log_weight = (beyond + own_total)[:, None, :] - running + input_pre
    stabilizer = lax.pmax(jnp.max(log_weight, axis=1), "sp")
    weight = jnp.exp(log_weight - stabilizer[:, None, :])
    key_heads = key_rows.reshape(seq_count, span, head_count, DH)
    value_heads = value_rows.reshape(seq_count, span, head_count, DH)
    weighted = (weight[..., None] * value_heads.astype(jnp.float32)).astype(jnp.bfloat16)
    partial_normal = jnp.einsum("sth,sthd->shd", weight, key_heads.astype(jnp.float32))
    partial_matrix = jnp.einsum(
        "sthe,sthd->shed", weighted, key_heads, preferred_element_type=jnp.float32
    )
    matrix, normal = (
        lax.psum_scatter(partial_matrix, "sp", scatter_dimension=2, tiled=True),
        lax.psum_scatter(partial_normal, "sp", scatter_dimension=2, tiled=True),
    )
    cache_matrix = matrix.astype(jnp.bfloat16)
    new_normed = normalize(lax.all_gather(new_rows, "tp", axis=1, tiled=True))
    query_new = jnp.dot(new_normed, w_query, preferred_element_type=jnp.float32).astype(
        jnp.bfloat16
    )
    key_new = jnp.dot(new_normed, w_key, preferred_element_type=jnp.float32).astype(jnp.bfloat16)
    value_new = jnp.dot(new_normed, w_value, preferred_element_type=jnp.float32).astype(
        jnp.bfloat16
    )
    query_new = query_new.astype(jnp.float32).reshape(seq_count, head_count, DH)
    key_new = key_new.astype(jnp.float32).reshape(seq_count, head_count, DH)
    value_new = value_new.astype(jnp.float32).reshape(seq_count, head_count, DH)
    value_own = lax.dynamic_slice_in_dim(value_new, row_start, rows_own, 2)
    query_own = lax.dynamic_slice_in_dim(query_new, row_start, rows_own, 2)
    input_new = jnp.dot(new_normed, gate_in, preferred_element_type=jnp.float32)
    forget_new = jax.nn.log_sigmoid(
        jnp.dot(new_normed, gate_forget, preferred_element_type=jnp.float32) + bias_heads
    )
    top_next = jnp.maximum(forget_new + stabilizer, input_new)
    old_share = jnp.exp(forget_new + stabilizer - top_next)
    new_share = jnp.exp(input_new - top_next)
    agreement = jnp.sum(key_new * query_new, axis=-1)
    factor = DH ** (-0.5)
    numerator = old_share[..., None] * jnp.einsum(
        "shed,shd->she", cache_matrix.astype(jnp.float32), query_new
    )
    numerator = (numerator + (new_share * agreement)[..., None] * value_own) * factor
    normal_dot = lax.psum(jnp.sum(normal * query_own, axis=-1), "sp")
    denominator = (old_share * normal_dot + new_share * agreement) * factor
    read = numerator / jnp.maximum(jnp.abs(denominator), 1.0)[..., None]
    return (cache_matrix, normal, stabilizer, read.astype(jnp.bfloat16))


def solution(mesh):
    in_specs = (
        P(None, "sp", None),
        P(None, "tp"),
        P(None, "tp"),
        P(None, "tp"),
        P(),
        P(),
        P(),
        P(None, "tp"),
    )
    out_specs = (P(None, "tp", "sp", None), P(None, "tp", "sp"), P(None, "tp"), P(None, "tp", "sp"))
    return jax.shard_map(shards, mesh=mesh, in_specs=in_specs, out_specs=out_specs, check_vma=False)
```

profile of v0, /device:TPU:0, one launch (start us, length us, event | category | flops | bytes accessed | tf_op | source)
XLA Modules:
  0.0 208.2 jit_solution(13657243341448075160)
XLA Ops:
  7.3 4.1 %fusion = f32[2,384]{1,0:T(2,128)S(1)} fusion(bf16[2,384,4096]{2,1,0:T(8,128)(2,1)} %param.10), kind=kLoop, calls=%fused_computation.3 | loop fusion | flops 9436416 | bytes 6294528 | tf_op jit(solution)/shard_map/reduce_sum | solution.py:26
  11.5 4.6 %fusion.64 = f32[2,4,3,128]{3,1,2,0:T(4,128)S(1)} fusion(bf16[4096,16]{0,1:T(8,128)(2,1)S(1)} %copy-done, s32[]{:T(128)S(6)} %select_n.52, bf16[2,384,4096]{2,1,0:T(8,128)(2,1)} %param.10, f32[2,384]{1,0:T(2,128)S(1)} %add_rsqrt_fusion, f32[4]{0:T(128)S(1)} %dynamic_slice.26), kind=kOutput, calls=%fused_computation.47 | convolution fusion | flops 34630656 | bytes 6340100 | tf_op jit(solution)/shard_map/spd,dh->sph/dot_general | solution.py:52
  16.1 2.4 %reduce-window.6 = f32[2,4,3,128]{3,2,1,0:T(4,128)S(1)} reduce-window(f32[2,4,3,128]{3,2,1,0:T(4,128)S(1)} %copy.21, f32[]{:T(128)} %constant.74.clone.1), window={size=1x1x1x128 pad=0_0x0_0x0_0x127_0}, to_apply=%region_1.2 | reduce-window | flops 390144 | bytes 24580 | tf_op jit(solution)/shard_map/reduce-window
  18.6 0.1 copy.22
  19.0 0.2 slice_reduce_fusion
  19.2 22.3 %all-gather = f32[16,1,4]{2,1,0:T(1,128)S(1)} all-gather(f32[2,1,4]{2,1,0:T(1,128)S(1)} %copy.24), channel_id=2, replica_groups=mesh['sp'=8,'tp'=4] {'sp'}, dimensions={0}, use_global_device_ids=true | all-gather | bytes 288 | tf_op jit(solution)/shard_map/all_gather | solution.py:12
  41.5 0.3 while.16
  41.8 4.7 %fusion.91 = (f32[2,4]{1,0:T(2,128)S(1)}, f32[2,384,4]{1,2,0:T(4,128)S(1)}) fusion(bf16[4096,16]{0,1:T(8,128)(2,1)S(1)} %copy-done.6, s32[]{:T(128)S(6)} %select_n.52, bf16[2,384,4096]{2,1,0:T(8,128)(2,1)} %param.10, f32[2,384]{1,0:T(2,128)S(1)} %add_rsqrt_fusion, f32[2,4,384]{2,1,0:T(4,128)S(1)} %reduce_window_sum.16, f32[2,4]{1,0:T(2,128)S(1)} %add.125), kind=kOutput, calls=%fused_computation.73 | convolution fusion | flops 34612216 | bytes 6352932 | tf_op jit(solution)/shard_map/spd,dh->sph/dot_general | solution.py:50
  46.5 17.1 %pmax.7 = f32[2,4]{1,0:T(2,128)S(1)} all-reduce(f32[2,4]{1,0:T(2,128)S(1)} %get-tuple-element.143), channel_id=1, replica_groups=mesh['sp'=8,'tp'=4] {'sp'}, use_global_device_ids=true, to_apply=%region_6.7 | all-reduce | flops 8 | bytes 64 | tf_op jit(solution)/shard_map/pmax | solution.py:59
  63.6 7.5 %fusion.27 = bf16[2,48,4,8,128]{4,3,2,1,0:T(8,128)(2,1)S(1)} fusion(bf16[4096,512]{1,0:T(8,128)(2,1)} %param.11, bf16[2,384,4096]{2,1,0:T(8,128)(2,1)} %param.10, f32[2,384]{1,0:T(2,128)S(1)} %add_rsqrt_fusion), kind=kOutput, calls=%fused_computation.15 | convolution fusion | flops 3231055872 | bytes 11275264 | tf_op jit(solution)/shard_map/spd,dc->spc/dot_general | solution.py:44
  71.2 0.8 copy-done.1
  72.0 0.2 fusion.48
  72.2 0.2 copy.32
  72.4 0.7 reshape.91
  73.3 6.9 %fusion.17 = f32[2,384,512]{2,1,0:T(8,128)S(1)} fusion(bf16[4096,512]{1,0:T(8,128)(2,1)} %param.12, bf16[2,384,4096]{2,1,0:T(8,128)(2,1)} %param.10, f32[2,384]{1,0:T(2,128)S(1)} %add_rsqrt_fusion), kind=kOutput, calls=%fused_computation.13 | convolution fusion | flops 3231449088 | bytes 12061696 | tf_op jit(solution)/shard_map/spd,dc->spc/dot_general | solution.py:47
  80.2 0.5 copy.31
  80.7 2.3 %fusion.47 = f32[2,4,128,128]{3,2,1,0:T(8,128)} fusion(f32[2,384,4,128]{1,3,2,0:T(8,128)S(1)} %bitcast.61, f32[2,384,4]{1,2,0:T(4,128)S(1)} %subtract_exponential_fusion, bf16[2,48,4,8,128]{4,3,2,1,0:T(8,128)(2,1)} %copy-done.1), kind=kOutput, calls=%fused_computation.27 | convolution fusion | flops 101449728 | bytes 2895872 | tf_op jit(solution)/shard_map/sthe,sthd->shed/dot_general | solution.py:65
  83.0 5.2 %all_gather.7 = bf16[2,4096]{1,0:T(2,128)(2,1)S(1)} all-gather(bf16[2,1024]{1,0:T(2,128)(2,1)S(1)} %copy-done.5), channel_id=1, replica_groups=mesh['sp'=8,'tp'=4] {'tp'}, dimensions={1}, use_global_device_ids=true | all-gather | bytes 20480 | tf_op jit(solution)/shard_map/all_gather | solution.py:73
  88.2 0.1 fusion.54
  88.4 2.9 %fusion.45 = f32[2,512]{1,0:T(2,128)S(1)} fusion(bf16[4096,512]{1,0:T(8,128)(2,1)} %param.11, bf16[2,4096]{1,0:T(2,128)(2,1)S(1)} %all_gather.7, f32[2]{0:T(128)S(1)} %add_rsqrt_fusion.1), kind=kOutput, calls=%fused_computation.23 | convolution fusion | flops 8415232 | bytes 4214792 | tf_op jit(solution)/shard_map/dot_general | solution.py:77
  91.3 2.9 %convolution_convert_fusion.2 = bf16[2,512]{1,0:T(2,128)(2,1)S(1)} fusion(bf16[4096,512]{1,0:T(8,128)(2,1)} %param.13, bf16[2,4096]{1,0:T(2,128)(2,1)S(1)} %all_gather.7, f32[2]{0:T(128)S(1)} %add_rsqrt_fusion.1), kind=kOutput, calls=%fused_computation.24 | convolution fusion | flops 8414208 | bytes 4212744 | tf_op jit(solution)/shard_map/dot_general | solution.py:74
  94.3 0.2 fusion.58
  94.5 2.9 %fusion.44 = f32[2,512]{1,0:T(2,128)S(1)} fusion(bf16[4096,512]{1,0:T(8,128)(2,1)} %param.12, bf16[2,4096]{1,0:T(2,128)(2,1)S(1)} %all_gather.7, f32[2]{0:T(128)S(1)} %add_rsqrt_fusion.1), kind=kOutput, calls=%fused_computation.21 | convolution fusion | flops 8415232 | bytes 4214792 | tf_op jit(solution)/shard_map/dot_general | solution.py:78
  97.4 37.1 %reduce-scatter.7.cloned.1.call-done = f32[16,8]{1,0:T(8,128)} async-done(((f32[128,8]{1,0:T(8,128)}), f32[16,8]{1,0:T(8,128)}) %reduce-scatter.7.cloned.1.call-update) | async-done | bytes 528
  134.6 0.8 reshape.92
  135.4 0.2 multiply_reduce_fusion
  135.6 19.5 %psum.7 = f32[2,4]{1,0:T(2,128)S(1)} all-reduce(f32[2,4]{1,0:T(2,128)S(1)} %multiply_reduce_fusion), channel_id=1, replica_groups=mesh['sp'=8,'tp'=4] {'sp'}, use_global_device_ids=true, to_apply=%region_12.13 | all-reduce | flops 8 | bytes 64 | tf_op jit(solution)/shard_map/psum | solution.py:99
  155.1 0.2 abs_maximum_fusion
  155.4 44.3 %reduce-scatter.5.cloned.1.call-done = f32[2,4,16,128]{3,2,1,0:T(8,128)} async-done(((f32[2,4,128,128]{3,2,1,0:T(8,128)}), f32[2,4,16,128]{3,2,1,0:T(8,128)}) %reduce-scatter.5.cloned.1.call-update) | async-done | bytes 65552 | tf_op jit(solution)/shard_map/reduce_scatter | solution.py:69
  199.7 0.8 convert_element_type.54
  200.5 0.1 fusion.92
  200.6 0.7 fusion.70
  (49 shorter events, 1.2 us)
Async XLA Ops:
  7.2 4.3 %copy-start = (bf16[4096,16]{0,1:T(8,128)(2,1)S(1)}, bf16[4096,16]{0,1:T(8,128)(2,1)}, u32[]{:S(2)}) copy-start(bf16[4096,16]{0,1:T(8,128)(2,1)} %param.15) | copy-start | bytes 393220
  7.2 4.2 %copy-start.7 = (f32[16]{0:T(128)S(1)}, f32[16]{0:T(128)}, u32[]{:S(2)}) copy-start(f32[16]{0:T(128)} %param.16) | copy-start | bytes 196
  7.2 127.4 %reduce-scatter.7.cloned.1.call-start = ((), (), s32[]{:S(2)}) async-start(), calls=%async_computation.3 | async-start | bytes 73728
  7.2 34.6 %copy-start.6 = (bf16[4096,16]{0,1:T(8,128)(2,1)S(1)}, bf16[4096,16]{0,1:T(8,128)(2,1)}, u32[]{:S(2)}) copy-start(bf16[4096,16]{0,1:T(8,128)(2,1)} %param.14) | copy-start | bytes 393220
  63.6 91.5 %copy-start.4 = (f32[2,4]{1,0:T(2,128)}, f32[2,4]{1,0:T(2,128)S(1)}, u32[]{:S(2)}) copy-start(f32[2,4]{1,0:T(2,128)S(1)} %pmax.7) | copy-start | bytes 100
  71.1 0.9 copy-start.1
  73.2 126.5 %reduce-scatter.5.cloned.1.call-start = ((), (), s32[]{:S(2)}) async-start(), calls=%async_computation.2 | async-start | bytes 589824 | tf_op jit(solution)/shard_map/reduce_scatter | solution.py:69
  80.2 2.8 %copy-start.5 = (bf16[2,1024]{1,0:T(2,128)(2,1)S(1)}, bf16[2,1024]{1,0:T(2,128)(2,1)}, u32[]{:S(2)}) copy-start(bf16[2,1024]{1,0:T(2,128)(2,1)} %param.17) | copy-start | bytes 12292
  135.4 65.9 %copy-start.3 = (f32[2,4,16]{2,1,0:T(4,128)}, f32[2,4,16]{2,1,0:T(4,128)S(1)}, u32[]{:S(2)}) copy-start(f32[2,4,16]{2,1,0:T(4,128)S(1)} %copy.33) | copy-start | bytes 1540
  200.5 0.8 copy-start.2
Sparse Core Ops, SparseCore 0:
  73.3 61.2 reduce-scatter.6
  137.9 61.7 reduce-scatter.4
where the time goes:
time: 209 us; the launch traced here: 208 us
  waiting for transfers between devices  81.5 us (39%)
  blocking collectives  64.1 us (31%)
  matrix products  35.4 us (17%)
  between operations  14.2 us (7%)
  other arithmetic  8.84 us (4%)
  local copies, waits for them, and re-layouts  3.79 us (2%)
    reduce_scatter x1, waiting for transfers between devices, shards(): lax.psum_scatter(partial_matrix, 'sp', scatter_dimension=2, tiled=True)  44.3 us
    unnamed x3, waiting for transfers between devices  37.2 us
    all_gather x1, blocking collectives, prefix(): everything = lax.all_gather(value, axis)  22.3 us
    psum x1, blocking collectives, shards(): normal_dot = lax.psum(jnp.sum(normal * query_own, axis=-1), 'sp')  19.5 us
    pmax x1, blocking collectives, shards(): stabilizer = lax.pmax(jnp.max(log_weight, axis=1), 'sp')  17.1 us
    dot_general x1, matrix products, shards(): jnp.einsum('spd,dc->spc', normed, w_key, preferred_element_type=jnp.float32)  7.46 us
    dot_general x1, matrix products, shards(): jnp.einsum('spd,dc->spc', normed, w_value, preferred_element_type=jnp.flo...  6.89 us
    all_gather x1, blocking collectives, shards(): new_normed = normalize(lax.all_gather(new_rows, 'tp', axis=1, tiled=True))  5.21 us
  transfers between devices with their start and end apart: 2, of which 2 were waited for; matrix products, arithmetic and copies ran while one was open for 10% of the time, Pallas kernels for 0%

commit v1 on v0

--- a/solution.py
+++ b/solution.py
@@ -96,7 +96,7 @@
         "shed,shd->she", cache_matrix.astype(jnp.float32), query_new
     )
     numerator = (numerator + (new_share * agreement)[..., None] * value_own) * factor
-    normal_dot = lax.psum(jnp.sum(normal * query_own, axis=-1), "sp")
+    normal_dot = jnp.sum(lax.all_gather(jnp.sum(normal * query_own, axis=-1), "sp"), axis=0)
     denominator = (old_share * normal_dot + new_share * agreement) * factor
     read = numerator / jnp.maximum(jnp.abs(denominator), 1.0)[..., None]
     return (cache_matrix, normal, stabilizer, read.astype(jnp.bfloat16))

time: 209 us -> 209 us (level)
    psum x1 -> x0, blocking collectives: 19.5 us -> none  [shards(): normal_dot = lax.psum(jnp.sum(normal * query_own, axis=-1), 'sp')]
    all_gather x0 -> x1, blocking collectives: none -> 18.6 us  [shards(): lax.all_gather(jnp.sum(normal * query_own, axis=-1), 'sp')]
where the time goes in v1:
time: 209 us; the launch traced here: 208 us
  waiting for transfers between devices  82.3 us (39%)
  blocking collectives  63.3 us (30%)
  matrix products  35.4 us (17%)
  between operations  14.2 us (7%)
  other arithmetic  8.86 us (4%)
  local copies, waits for them, and re-layouts  3.79 us (2%)
    reduce_scatter x1, waiting for transfers between devices, shards(): lax.psum_scatter(partial_matrix, 'sp', scatter_dimension=2, tiled=True)  45.2 us
    unnamed x3, waiting for transfers between devices  37.2 us
    all_gather x1, blocking collectives, prefix(): everything = lax.all_gather(value, axis)  22.3 us
    all_gather x1, blocking collectives, shards(): lax.all_gather(jnp.sum(normal * query_own, axis=-1), 'sp')  18.6 us
    pmax x1, blocking collectives, shards(): stabilizer = lax.pmax(jnp.max(log_weight, axis=1), 'sp')  17.1 us
    dot_general x1, matrix products, shards(): jnp.einsum('spd,dc->spc', normed, w_key, preferred_element_type=jnp.float32)  7.46 us
    dot_general x1, matrix products, shards(): jnp.einsum('spd,dc->spc', normed, w_value, preferred_element_type=jnp.flo...  6.89 us
    all_gather x1, blocking collectives, shards(): new_normed = normalize(lax.all_gather(new_rows, 'tp', axis=1, tiled=True))  5.21 us
  transfers between devices with their start and end apart: 2, of which 2 were waited for; matrix products, arithmetic and copies ran while one was open for 10% of the time, Pallas kernels for 0%

profile of v1, /device:TPU:0, one launch (start us, length us, event | category | flops | bytes accessed | tf_op | source)
XLA Modules:
  0.0 208.1 jit_solution(15284433392969613356)
XLA Ops:
  7.3 4.1 %fusion = f32[2,384]{1,0:T(2,128)S(1)} fusion(bf16[2,384,4096]{2,1,0:T(8,128)(2,1)} %param.10), kind=kLoop, calls=%fused_computation.3 | loop fusion | flops 9436416 | bytes 6294528 | tf_op jit(solution)/shard_map/reduce_sum | solution.py:26
  11.5 4.6 %fusion.64 = f32[2,4,3,128]{3,1,2,0:T(4,128)S(1)} fusion(bf16[4096,16]{0,1:T(8,128)(2,1)S(1)} %copy-done, s32[]{:T(128)S(6)} %select_n.52, bf16[2,384,4096]{2,1,0:T(8,128)(2,1)} %param.10, f32[2,384]{1,0:T(2,128)S(1)} %add_rsqrt_fusion, f32[4]{0:T(128)S(1)} %dynamic_slice.26), kind=kOutput, calls=%fused_computation.47 | convolution fusion | flops 34630656 | bytes 6340100 | tf_op jit(solution)/shard_map/spd,dh->sph/dot_general | solution.py:52
  16.1 2.4 %reduce-window.6 = f32[2,4,3,128]{3,2,1,0:T(4,128)S(1)} reduce-window(f32[2,4,3,128]{3,2,1,0:T(4,128)S(1)} %copy.21, f32[]{:T(128)} %constant.74.clone.1), window={size=1x1x1x128 pad=0_0x0_0x0_0x127_0}, to_apply=%region_1.2 | reduce-window | flops 390144 | bytes 24580 | tf_op jit(solution)/shard_map/reduce-window
  18.6 0.1 copy.22
  19.0 0.2 slice_reduce_fusion
  19.2 22.3 %all-gather = f32[16,1,4]{2,1,0:T(1,128)S(1)} all-gather(f32[2,1,4]{2,1,0:T(1,128)S(1)} %copy.24), channel_id=2, replica_groups=mesh['sp'=8,'tp'=4] {'sp'}, dimensions={0}, use_global_device_ids=true | all-gather | bytes 288 | tf_op jit(solution)/shard_map/all_gather | solution.py:12
  41.5 0.3 while.16
  41.8 4.7 %fusion.91 = (f32[2,4]{1,0:T(2,128)S(1)}, f32[2,384,4]{1,2,0:T(4,128)S(1)}) fusion(bf16[4096,16]{0,1:T(8,128)(2,1)S(1)} %copy-done.6, s32[]{:T(128)S(6)} %select_n.52, bf16[2,384,4096]{2,1,0:T(8,128)(2,1)} %param.10, f32[2,384]{1,0:T(2,128)S(1)} %add_rsqrt_fusion, f32[2,4,384]{2,1,0:T(4,128)S(1)} %reduce_window_sum.16, f32[2,4]{1,0:T(2,128)S(1)} %add.123), kind=kOutput, calls=%fused_computation.73 | convolution fusion | flops 34612216 | bytes 6352932 | tf_op jit(solution)/shard_map/spd,dh->sph/dot_general | solution.py:50
  46.5 17.1 %pmax.7 = f32[2,4]{1,0:T(2,128)S(1)} all-reduce(f32[2,4]{1,0:T(2,128)S(1)} %get-tuple-element.143), channel_id=1, replica_groups=mesh['sp'=8,'tp'=4] {'sp'}, use_global_device_ids=true, to_apply=%region_6.7 | all-reduce | flops 8 | bytes 64 | tf_op jit(solution)/shard_map/pmax | solution.py:59
  63.6 7.5 %fusion.27 = bf16[2,48,4,8,128]{4,3,2,1,0:T(8,128)(2,1)S(1)} fusion(bf16[4096,512]{1,0:T(8,128)(2,1)} %param.11, bf16[2,384,4096]{2,1,0:T(8,128)(2,1)} %param.10, f32[2,384]{1,0:T(2,128)S(1)} %add_rsqrt_fusion), kind=kOutput, calls=%fused_computation.15 | convolution fusion | flops 3231055872 | bytes 11275264 | tf_op jit(solution)/shard_map/spd,dc->spc/dot_general | solution.py:44
  71.2 0.8 copy-done.1
  72.0 0.2 fusion.48
  72.2 0.2 copy.32
  72.4 0.7 reshape.95
  73.3 6.9 %fusion.17 = f32[2,384,512]{2,1,0:T(8,128)S(1)} fusion(bf16[4096,512]{1,0:T(8,128)(2,1)} %param.12, bf16[2,384,4096]{2,1,0:T(8,128)(2,1)} %param.10, f32[2,384]{1,0:T(2,128)S(1)} %add_rsqrt_fusion), kind=kOutput, calls=%fused_computation.13 | convolution fusion | flops 3231449088 | bytes 12061696 | tf_op jit(solution)/shard_map/spd,dc->spc/dot_general | solution.py:47
  80.2 0.5 copy.31
  80.7 2.3 %fusion.47 = f32[2,4,128,128]{3,2,1,0:T(8,128)} fusion(f32[2,384,4,128]{1,3,2,0:T(8,128)S(1)} %bitcast.62, f32[2,384,4]{1,2,0:T(4,128)S(1)} %subtract_exponential_fusion, bf16[2,48,4,8,128]{4,3,2,1,0:T(8,128)(2,1)} %copy-done.1), kind=kOutput, calls=%fused_computation.27 | convolution fusion | flops 101449728 | bytes 2895872 | tf_op jit(solution)/shard_map/sthe,sthd->shed/dot_general | solution.py:65
  83.0 5.2 %all_gather.13 = bf16[2,4096]{1,0:T(2,128)(2,1)S(1)} all-gather(bf16[2,1024]{1,0:T(2,128)(2,1)S(1)} %copy-done.5), channel_id=1, replica_groups=mesh['sp'=8,'tp'=4] {'tp'}, dimensions={1}, use_global_device_ids=true | all-gather | bytes 20480 | tf_op jit(solution)/shard_map/all_gather | solution.py:73
  88.2 0.1 fusion.54
  88.4 2.9 %fusion.44 = f32[2,512]{1,0:T(2,128)S(1)} fusion(bf16[4096,512]{1,0:T(8,128)(2,1)} %param.12, bf16[2,4096]{1,0:T(2,128)(2,1)S(1)} %all_gather.13, f32[2]{0:T(128)S(1)} %add_rsqrt_fusion.1), kind=kOutput, calls=%fused_computation.21 | convolution fusion | flops 8415232 | bytes 4214792 | tf_op jit(solution)/shard_map/dot_general | solution.py:78
  91.3 2.9 %convolution_convert_fusion.2 = bf16[2,512]{1,0:T(2,128)(2,1)S(1)} fusion(bf16[4096,512]{1,0:T(8,128)(2,1)} %param.13, bf16[2,4096]{1,0:T(2,128)(2,1)S(1)} %all_gather.13, f32[2]{0:T(128)S(1)} %add_rsqrt_fusion.1), kind=kOutput, calls=%fused_computation.24 | convolution fusion | flops 8414208 | bytes 4212744 | tf_op jit(solution)/shard_map/dot_general | solution.py:74
  94.2 2.9 %fusion.45 = f32[2,512]{1,0:T(2,128)S(1)} fusion(bf16[4096,512]{1,0:T(8,128)(2,1)} %param.11, bf16[2,4096]{1,0:T(2,128)(2,1)S(1)} %all_gather.13, f32[2]{0:T(128)S(1)} %add_rsqrt_fusion.1), kind=kOutput, calls=%fused_computation.23 | convolution fusion | flops 8415232 | bytes 4214792 | tf_op jit(solution)/shard_map/dot_general | solution.py:77
  97.2 0.2 fusion.58
  97.4 37.1 %reduce-scatter.7.cloned.1.call-done = f32[16,8]{1,0:T(8,128)} async-done(((f32[128,8]{1,0:T(8,128)}), f32[16,8]{1,0:T(8,128)}) %reduce-scatter.7.cloned.1.call-update) | async-done | bytes 528
  134.6 0.8 reshape.96
  135.4 0.2 multiply_reduce_fusion
  135.6 18.6 %all-gather.2 = f32[8,2,4]{2,1,0:T(2,128)S(1)} all-gather(f32[1,2,4]{2,1,0:T(2,128)S(1)} %bitcast.69), channel_id=3, replica_groups=mesh['sp'=8,'tp'=4] {'sp'}, dimensions={0}, use_global_device_ids=true | all-gather | bytes 288 | tf_op jit(solution)/shard_map/all_gather | solution.py:99
  154.2 0.2 abs_maximum_fusion
  154.5 45.2 %reduce-scatter.5.cloned.1.call-done = f32[2,4,16,128]{3,2,1,0:T(8,128)} async-done(((f32[2,4,128,128]{3,2,1,0:T(8,128)}), f32[2,4,16,128]{3,2,1,0:T(8,128)}) %reduce-scatter.5.cloned.1.call-update) | async-done | bytes 65552 | tf_op jit(solution)/shard_map/reduce_scatter | solution.py:69
  199.6 0.8 convert_element_type.54
  200.5 0.1 fusion.92
  200.6 0.7 fusion.70
  (50 shorter events, 1.2 us)
Async XLA Ops:
  7.2 4.3 %copy-start = (bf16[4096,16]{0,1:T(8,128)(2,1)S(1)}, bf16[4096,16]{0,1:T(8,128)(2,1)}, u32[]{:S(2)}) copy-start(bf16[4096,16]{0,1:T(8,128)(2,1)} %param.15) | copy-start | bytes 393220
  7.2 4.2 %copy-start.7 = (f32[16]{0:T(128)S(1)}, f32[16]{0:T(128)}, u32[]{:S(2)}) copy-start(f32[16]{0:T(128)} %param.16) | copy-start | bytes 196
  7.2 127.4 %reduce-scatter.7.cloned.1.call-start = ((), (), s32[]{:S(2)}) async-start(), calls=%async_computation.3 | async-start | bytes 73728
  7.2 34.6 %copy-start.6 = (bf16[4096,16]{0,1:T(8,128)(2,1)S(1)}, bf16[4096,16]{0,1:T(8,128)(2,1)}, u32[]{:S(2)}) copy-start(bf16[4096,16]{0,1:T(8,128)(2,1)} %param.14) | copy-start | bytes 393220
  63.6 90.6 %copy-start.4 = (f32[2,4]{1,0:T(2,128)}, f32[2,4]{1,0:T(2,128)S(1)}, u32[]{:S(2)}) copy-start(f32[2,4]{1,0:T(2,128)S(1)} %pmax.7) | copy-start | bytes 100
  71.1 0.9 copy-start.1
  73.2 126.5 %reduce-scatter.5.cloned.1.call-start = ((), (), s32[]{:S(2)}) async-start(), calls=%async_computation.2 | async-start | bytes 589824 | tf_op jit(solution)/shard_map/reduce_scatter | solution.py:69
  80.2 2.8 %copy-start.5 = (bf16[2,1024]{1,0:T(2,128)(2,1)S(1)}, bf16[2,1024]{1,0:T(2,128)(2,1)}, u32[]{:S(2)}) copy-start(bf16[2,1024]{1,0:T(2,128)(2,1)} %param.17) | copy-start | bytes 12292
  135.4 65.8 %copy-start.3 = (f32[2,4,16]{2,1,0:T(4,128)}, f32[2,4,16]{2,1,0:T(4,128)S(1)}, u32[]{:S(2)}) copy-start(f32[2,4,16]{2,1,0:T(4,128)S(1)} %copy.33) | copy-start | bytes 1540
  200.5 0.8 copy-start.2
Sparse Core Ops, SparseCore 0:
  73.3 61.2 reduce-scatter.6
  137.9 61.6 reduce-scatter.4
